TPU v7x, 32 devices: a whole 2x2x4 slice. The times are simulated.
32 devices in a mesh: ep: 4 (over y, x), tp: 8 (over z, core).
Axes of the slice: x: 2, y: 2, z: 4, core: 2. Of those that a mesh axis runs over, the one named last changes fastest.
Arguments:
- tokens: bfloat16 [64, 2048], P('ep', 'tp'), may hold values from -6 to 6
- key_cache: bfloat16 [64, 16, 1024, 128], P('ep', 'tp'), may hold values from -1700 to 1700
- value_cache: bfloat16 [64, 16, 1024, 128], P('ep', 'tp'), may hold values from -6 to 6
- gate_totals: float32 [64, 16, 1024], P('ep', 'tp'), as said below
- lengths: int32 [64], P('ep'), may hold values from 128 to 1024
- attn_gain: float32 [2048], replicated, may hold values from 0.1 to 1.9
- w_query: bfloat16 [2048, 2048], P(None, 'tp'), may hold values from -0.125 to 0.125
- w_key: bfloat16 [2048, 2048], P(None, 'tp'), may hold values from -0.125 to 0.125
- w_value: bfloat16 [2048, 2048], P(None, 'tp'), may hold values from -0.125 to 0.125
- w_forget: bfloat16 [2048, 16], replicated, may hold values from -0.125 to 0.125
- forget_bias: float32 [16], replicated, may hold values from -3 to 0
- w_attn_out: bfloat16 [2048, 2048], P('tp'), may hold values from -0.1875 to 0.1875
- moe_gain: float32 [2048], replicated, may hold values from 0.1 to 1.9
- group_ids: int32 [64, 1], P('ep'), may hold values from 0 to 3; in each aligned block of 16 rows (0 to 15, 16 to 31, ...) at most 8 rows name the same one
- inner_ids: int32 [64, 2], P('ep'), may hold values from 0 to 3, all different within a row
- group_prob: float32 [64], P('ep'), may hold values from 0.2 to 1
- pair_logits: float32 [64, 2], P('ep'), may hold values from -6 to 6
- w_expert_gate: bfloat16 [4, 2048, 2048], P('ep', None, 'tp'), may hold values from -0.125 to 0.125
- w_expert_up: bfloat16 [4, 2048, 2048], P('ep', None, 'tp'), may hold values from -0.125 to 0.125
- w_expert_down: bfloat16 [4, 2048, 2048], P('ep', 'tp'), may hold values from -0.375 to 0.375
- w_dense_in: bfloat16 [2048, 2048], P(None, 'tp'), may hold values from -0.125 to 0.125
- w_dense_out: bfloat16 [2048, 2048], P('tp'), may hold values from -0.1875 to 0.1875
- dense_gate: float32 [2048], P('tp'), may hold values from -2 to 2
Outputs:
- layer_output: bfloat16 [64, 2048], P('ep', 'tp')
- new_keys: bfloat16 [64, 16, 128], P('ep', 'tp')
- new_values: bfloat16 [64, 16, 128], P('ep', 'tp')
- new_gates: float32 [64, 16], P('ep', 'tp')
Inputs may be any that keep to these rules, and one draw needn't show every extreme that they name: `group_ids`: within the 16 sequences of each index of ep (aligned blocks of rows), no group is named by more than 8 sequences, a bound that some block reaches. `inner_ids`: each row names 2 different experts of its group. `gate_totals`: along positions the values of each sequence and head never rise.
All inputs are finite; a program needn't handle non-finite values.
Results may differ from a plain program's by a relative error of at most 0.011.
Values may be sent and summed in bfloat16 or wider, within the bound.
A program may use at most 64 MiB of HBM per device.

v0:
```python
import jax
import jax.numpy as jnp
from jax import lax
from jax.sharding import PartitionSpec as P

FFE = 512
EPG = 4
EPS = 1e-06
FLOOR = -1e30


def norm_rows(row_data, gain_vec):
    values = row_data.astype(jnp.float32)
    factor = lax.rsqrt(jnp.mean(values * values, axis=-1, keepdims=True) + EPS)
    return (values * factor * gain_vec).astype(jnp.bfloat16)


def head_norm(values):
    factor = lax.rsqrt(jnp.mean(values * values, axis=-1, keepdims=True) + EPS)
    return (values * factor).astype(jnp.bfloat16)


def attend(queries, fresh_key, fresh_value, key_cache, value_cache, gate_totals, lengths, current):
    score_scale = queries.shape[-1] ** (-0.5)
    scores = (
        jnp.einsum("shd,shld->shl", queries, key_cache, preferred_element_type=jnp.float32)
        * score_scale
    )
    scores = scores + current[:, :, None] - gate_totals
    entry_indices = jnp.arange(key_cache.shape[2])
    live_mask = (entry_indices[None, :] < lengths[:, None])[:, None, :]
    scores = jnp.where(live_mask, scores, FLOOR)
    own_score = (
        jnp.sum(queries.astype(jnp.float32) * fresh_key.astype(jnp.float32), axis=-1) * score_scale
    )
    peak = jnp.maximum(jnp.max(scores, axis=-1), own_score)
    expo_terms = jnp.where(live_mask, jnp.exp(scores - peak[:, :, None]), 0.0)
    own_expo = jnp.exp(own_score - peak)
    denom_sum = jnp.sum(expo_terms, axis=-1) + own_expo
    weights = (expo_terms / denom_sum[:, :, None]).astype(jnp.bfloat16)
    own_weight = (own_expo / denom_sum).astype(jnp.bfloat16)
    attended = jnp.einsum("shl,shld->shd", weights, value_cache, preferred_element_type=jnp.float32)
    attended = attended + own_weight.astype(jnp.float32)[:, :, None] * fresh_value.astype(
        jnp.float32
    )
    return attended.astype(jnp.bfloat16)


def body(
    tokens,
    key_cache,
    value_cache,
    gate_totals,
    lengths,
    attn_gain,
    w_query,
    w_key,
    w_value,
    w_forget,
    forget_bias,
    w_attn_out,
    moe_gain,
    group_ids,
    inner_ids,
    group_prob,
    pair_logits,
    w_expert_gate,
    w_expert_up,
    w_expert_down,
    w_dense_in,
    w_dense_out,
    dense_gate,
):
    gathered = lax.all_gather(tokens, "tp", axis=1, tiled=True)
    normed = norm_rows(gathered, attn_gain)
    seq_count = gathered.shape[0]
    heads_dev = key_cache.shape[1]
    head_dim = key_cache.shape[3]

    def project(weight):
        return jnp.dot(normed, weight, preferred_element_type=jnp.float32).reshape(
            seq_count, heads_dev, head_dim
        )

    queries = head_norm(project(w_query))
    new_keys = head_norm(project(w_key))
    new_values = project(w_value).astype(jnp.bfloat16)
    first_head = lax.axis_index("tp") * heads_dev
    forget_cols = lax.dynamic_slice_in_dim(w_forget, first_head, heads_dev, 1)
    forget_shift = lax.dynamic_slice_in_dim(forget_bias, first_head, heads_dev, 0)
    log_gate = jax.nn.log_sigmoid(
        jnp.dot(normed, forget_cols, preferred_element_type=jnp.float32) + forget_shift
    )
    entry_indices = jnp.arange(gate_totals.shape[2])
    at_last = (entry_indices[None, :] == (lengths - 1)[:, None])[:, None, :]
    new_gates = jnp.sum(jnp.where(at_last, gate_totals, 0.0), axis=2) + log_gate
    attended = attend(
        queries, new_keys, new_values, key_cache, value_cache, gate_totals, lengths, new_gates
    )
    partial_value = jnp.dot(
        attended.reshape(seq_count, heads_dev * head_dim),
        w_attn_out,
        preferred_element_type=jnp.float32,
    )
    piece_sum = lax.psum_scatter(partial_value, "tp", scatter_dimension=1, tiled=True)
    own_residual = (tokens.astype(jnp.float32) + piece_sum).astype(jnp.bfloat16)
    moe_in = norm_rows(lax.all_gather(own_residual, "tp", axis=1, tiled=True), moe_gain)
    groups = lax.axis_size("ep")
    capacity = max(2, 2 * seq_count // groups)
    first_share = jax.nn.sigmoid(pair_logits[:, 0] - pair_logits[:, 1])
    pair_share = group_prob[:, None] * jnp.stack([first_share, 1.0 - first_share], axis=1)
    inner_range = jnp.arange(EPG)
    spread = jnp.sum(
        jnp.where(inner_ids[:, :, None] == inner_range[None, None, :], pair_share[:, :, None], 0.0),
        axis=1,
    ).astype(jnp.bfloat16)
    choose = (group_ids == jnp.arange(groups)[None, :]).astype(jnp.int32)
    before = jnp.cumsum(choose, axis=0) - choose
    slot_of = group_ids[:, 0] * capacity + jnp.sum(before * choose, axis=1)
    slot_ids = jnp.arange(groups * capacity)
    send_map = (slot_of[None, :] == slot_ids[:, None]).astype(jnp.bfloat16)
    send_weights = jnp.dot(send_map, spread, preferred_element_type=jnp.float32).astype(
        jnp.bfloat16
    )
    send_rows = jnp.dot(send_map, moe_in, preferred_element_type=jnp.float32).astype(jnp.bfloat16)
    recv_rows, recv_weights = (
        lax.all_to_all(send_rows, "ep", split_axis=0, concat_axis=0, tiled=True),
        lax.all_to_all(send_weights, "ep", split_axis=0, concat_axis=0, tiled=True),
    )
    dense_hidden = jax.nn.silu(
        jnp.dot(moe_in, w_dense_in, preferred_element_type=jnp.float32)
    ).astype(jnp.bfloat16)
    dense_part = jnp.dot(dense_hidden, w_dense_out, preferred_element_type=jnp.float32)
    hidden_dev = w_expert_gate.shape[2]
    expert_index = lax.axis_index("tp") * hidden_dev // FFE
    route_col = jnp.sum(
        jnp.where(inner_range[None, :] == expert_index, recv_weights.astype(jnp.float32), 0.0),
        axis=1,
    )
    gate_pre = jnp.dot(recv_rows, w_expert_gate[0], preferred_element_type=jnp.float32)
    up_pre = jnp.dot(recv_rows, w_expert_up[0], preferred_element_type=jnp.float32)
    hidden = (jax.nn.silu(gate_pre) * up_pre * route_col[:, None]).astype(jnp.bfloat16)
    expert_part = jnp.dot(hidden, w_expert_down[0], preferred_element_type=jnp.float32)
    expert_sum, dense_sum = (
        lax.psum_scatter(expert_part, "tp", scatter_dimension=1, tiled=True),
        lax.psum_scatter(dense_part, "tp", scatter_dimension=1, tiled=True),
    )
    returned = lax.all_to_all(
        expert_sum.astype(jnp.bfloat16), "ep", split_axis=0, concat_axis=0, tiled=True
    )
    expert_out = lax.dot_general(
        send_map, returned, (((0,), (0,)), ((), ())), preferred_element_type=jnp.float32
    )
    layer_output = (
        own_residual.astype(jnp.float32) + expert_out + jax.nn.sigmoid(dense_gate) * dense_sum
    )
    return (layer_output.astype(jnp.bfloat16), new_keys, new_values, new_gates)


def solution(mesh):
    placed = (
        P("ep", "tp"),
        P("ep", "tp", None, None),
        P("ep", "tp", None, None),
        P("ep", "tp", None),
        P("ep"),
        P(),
        P(None, "tp"),
        P(None, "tp"),
        P(None, "tp"),
        P(),
        P(),
        P("tp", None),
        P(),
        P("ep", None),
        P("ep", None),
        P("ep"),
        P("ep", None),
        P("ep", None, "tp"),
        P("ep", None, "tp"),
        P("ep", "tp", None),
        P(None, "tp"),
        P("tp", None),
        P("tp"),
    )
    return jax.shard_map(
        body,
        mesh=mesh,
        in_specs=placed,
        out_specs=(P("ep", "tp"), P("ep", "tp", None), P("ep", "tp", None), P("ep", "tp")),
        check_vma=False,
    )
```

profile of v0, /device:TPU:0, one launch (start us, length us, event | category | flops | bytes accessed | tf_op | source)
XLA Modules:
  0.0 172.8 jit_solution(14352880859179264883)
XLA Ops:
  7.3 0.8 broadcast_add_fusion
  8.1 0.7 iota_compare_fusion.1
  8.8 15.9 %all_gather.6 = bf16[16,2048]{1,0:T(8,128)(2,1)S(1)} all-gather(bf16[16,256]{1,0:T(8,128)(2,1)} %param.23), channel_id=1, replica_groups=mesh['ep'=4,'tp'=8] {'tp'}, dimensions={1}, use_global_device_ids=true | all-gather | bytes 73728 | tf_op jit(solution)/shard_map/all_gather | solution.py:74
  24.8 1.5 fusion.67
  26.5 1.5 fusion.70
  28.2 1.1 select_reduce_fusion
  29.4 0.7 dynamic_slice.7
  30.1 1.0 fusion.58
  31.2 0.7 multiply_reduce_fusion
  31.9 5.6 %fusion.34 = f32[16,2,1,1024]{3,2,1,0:T(1,128)S(1)} fusion(bf16[16,2,1024,128]{3,2,1,0:T(8,128)(2,1)} %param.24, bf16[16,2,128,1]{2,1,0,3:T(2,128)(2,1)S(1)} %get-tuple-element.12), kind=kOutput, calls=%fused_computation.48 | convolution fusion | flops 8388608 | bytes 8527872 | tf_op jit(solution)/shard_map/shd,shld->shl/dot_general | solution.py:26
  37.6 0.3 fusion.72
  37.9 0.3 fusion.32
  38.2 0.3 fusion.26
  38.5 0.3 convolution_convert_fusion.1
  38.9 4.7 %fusion.24 = f32[16,2,1,128]{3,2,1,0:T(1,128)S(1)} fusion(bf16[16,2,1024,128]{3,2,1,0:T(8,128)(2,1)} %param.25, bf16[16,2,1024,1]{2,1,0,3:T(2,128)(2,1)S(1)} %fusion.26), kind=kOutput, calls=%fused_computation.33 | convolution fusion | flops 8388608 | bytes 8470528 | tf_op jit(solution)/shard_map/shl,shld->shd/dot_general | solution.py:42
  43.7 2.1 %fusion.46 = f32[16,2048]{1,0:T(8,128)} fusion(bf16[256,2048]{1,0:T(8,128)(2,1)} %param.34, bf16[2,8,2,128]{3,2,1,0:T(2,128)(2,1)S(1)} %bitcast.56), kind=kOutput, calls=%fused_computation.66 | convolution fusion | flops 16777216 | bytes 1187840 | tf_op jit(solution)/shard_map/dot_general | solution.py:100
  46.4 0.6 copy.49
  47.0 3.7 %all-to-all-start.1 = ((bf16[4,8,4]{1,2,0:T(4,128)(2,1)}), bf16[4,8,4]{1,2,0:T(4,128)(2,1)S(1)}, u32[]{:S(2)}, u32[]{:S(2)}) async-start(bf16[4,8,4]{1,2,0:T(4,128)(2,1)} %copy.49), calls=%async_computation.2 | async-start | bytes 8192 | tf_op jit(solution)/shard_map/all_to_all | solution.py:128
  50.8 26.8 %reduce-scatter.4.cloned.1.call-done = f32[16,256]{1,0:T(8,128)} async-done(((f32[16,2048]{1,0:T(8,128)}), f32[16,256]{1,0:T(8,128)}) %reduce-scatter.4.cloned.1.call-update) | async-done | bytes 16400 | tf_op jit(solution)/shard_map/reduce_scatter | solution.py:105
  77.6 0.7 add_convert_fusion
  78.3 13.9 %all_gather.7 = bf16[16,2048]{1,0:T(8,128)(2,1)S(1)} all-gather(bf16[16,256]{1,0:T(8,128)(2,1)S(1)} %add_convert_fusion), channel_id=1, replica_groups=mesh['ep'=4,'tp'=8] {'tp'}, dimensions={1}, use_global_device_ids=true | all-gather | bytes 73728 | tf_op jit(solution)/shard_map/all_gather | solution.py:107
  92.4 0.9 fusion
  93.2 3.6 %all-to-all-start = ((bf16[4,8,2048]{2,1,0:T(8,128)(2,1)}), bf16[4,8,2048]{2,1,0:T(8,128)(2,1)S(1)}, u32[]{:S(2)}, u32[]{:S(2)}) async-start(bf16[4,8,2048]{2,1,0:T(8,128)(2,1)} %fusion), calls=%async_computation.1 | async-start | bytes 262144 | tf_op jit(solution)/shard_map/all_to_all | solution.py:127
  97.1 4.8 %all-to-all-done = bf16[4,8,2048]{2,1,0:T(8,128)(2,1)S(1)} async-done(((bf16[4,8,2048]{2,1,0:T(8,128)(2,1)}), bf16[4,8,2048]{2,1,0:T(8,128)(2,1)S(1)}, u32[]{:S(2)}, u32[]{:S(2)}) %all-to-all-start) | async-done | bytes 131104 | tf_op jit(solution)/shard_map/all_to_all | solution.py:127
  101.9 1.5 fusion.10
  103.4 2.7 %fusion.4 = f32[32,2048]{1,0:T(8,128)} fusion(bf16[1,256,2048]{2,1,0:T(8,128)(2,1)S(1)} %copy-done, bf16[1,2048,256]{2,1,0:T(8,128)(2,1)} %param.41, bf16[4,8,2048]{2,1,0:T(8,128)(2,1)S(1)} %all-to-all-done, f32[32,256]{1,0:T(8,128)S(1)} %fusion.10, f32[32]{0:T(128)S(1)} %mul.181), kind=kOutput, calls=%fused_computation.7 | convolution fusion | flops 67166208 | bytes 2523264 | tf_op jit(solution)/shard_map/dot_general | solution.py:143
  106.2 1.5 fusion.44
  107.7 26.1 %reduce-scatter.6.cloned.1.call-done = f32[32,256]{1,0:T(8,128)} async-done(((f32[32,2048]{1,0:T(8,128)}), f32[32,256]{1,0:T(8,128)}) %reduce-scatter.6.cloned.1.call-update) | async-done | bytes 32784 | tf_op jit(solution)/shard_map/reduce_scatter | solution.py:145
  133.7 1.4 convert_bitcast_fusion
  135.1 3.6 %all-to-all-start.2 = ((bf16[4,8,256]{2,1,0:T(8,128)(2,1)}), bf16[4,8,256]{2,1,0:T(8,128)(2,1)S(1)}, u32[]{:S(2)}, u32[]{:S(2)}) async-start(bf16[4,8,256]{2,1,0:T(8,128)(2,1)} %convert_bitcast_fusion), calls=%async_computation.4 | async-start | bytes 32768 | tf_op jit(solution)/shard_map/all_to_all | solution.py:148
  138.7 26.0 %reduce-scatter.8.cloned.1.call-done = f32[16,256]{1,0:T(8,128)} async-done(((f32[16,2048]{1,0:T(8,128)}), f32[16,256]{1,0:T(8,128)}) %reduce-scatter.8.cloned.1.call-update) | async-done | bytes 16400 | tf_op jit(solution)/shard_map/reduce_scatter | solution.py:146
  164.7 1.5 fusion.5
  (67 shorter events, 1.8 us)
Async XLA Ops:
  7.2 96.2 %copy-start = (bf16[1,256,2048]{2,1,0:T(8,128)(2,1)S(1)}, bf16[1,256,2048]{2,1,0:T(8,128)(2,1)}, u32[]{:S(2)}) copy-start(bf16[1,256,2048]{2,1,0:T(8,128)(2,1)} %param.42) | copy-start | bytes 3145732
  7.2 31.3 %copy-start.5 = (f32[2048]{0:T(1024)S(1)}, f32[2048]{0:T(1024)}, u32[]{:S(2)}) copy-start(f32[2048]{0:T(1024)} %param.28) | copy-start | bytes 24580
  7.2 30.3 %copy-start.4 = (f32[16,2,1024]{2,1,0:T(2,128)S(1)}, f32[16,2,1024]{2,1,0:T(2,128)}, u32[]{:S(2)}) copy-start(f32[16,2,1024]{2,1,0:T(2,128)} %param.26) | copy-start | bytes 393220
  7.2 31.3 %copy-start.3 = (bf16[2048,256]{1,0:T(8,128)(2,1)S(1)}, bf16[2048,256]{1,0:T(8,128)(2,1)}, u32[]{:S(2)}) copy-start(bf16[2048,256]{1,0:T(8,128)(2,1)} %param.31) | copy-start | bytes 3145732
  7.2 70.3 %reduce-scatter.4.cloned.1.call-start = ((), (), s32[]{:S(2)}) async-start(), calls=%async_computation.6 | async-start | bytes 147456 | tf_op jit(solution)/shard_map/reduce_scatter | solution.py:105
  31.1 12.5 %copy-start.11 = (f32[16,2]{0,1:T(2,128)}, f32[16,2]{0,1:T(2,128)S(1)}, u32[]{:S(2)}) copy-start(f32[16,2]{0,1:T(2,128)S(1)} %fusion.58) | copy-start | bytes 388
  37.5 8.3 %copy-start.9 = (s32[16,1]{0,1:T(1,128)S(1)}, s32[16,1]{0,1:T(1,128)}, u32[]{:S(2)}) copy-start(s32[16,1]{0,1:T(1,128)} %param.36) | copy-start | bytes 196
  37.5 8.6 %copy-start.12 = (f32[16,2]{0,1:T(2,128)S(1)}, f32[16,2]{0,1:T(2,128)}, u32[]{:S(2)}) copy-start(f32[16,2]{0,1:T(2,128)} %param.39) | copy-start | bytes 388
  37.6 8.6 %copy-start.14 = (f32[16]{0:T(128)S(1)}, f32[16]{0:T(128)}, u32[]{:S(2)}) copy-start(f32[16]{0:T(128)} %param.38) | copy-start | bytes 196
  37.6 8.6 %copy-start.10 = (s32[16,2]{0,1:T(2,128)S(1)}, s32[16,2]{0,1:T(2,128)}, u32[]{:S(2)}) copy-start(s32[16,2]{0,1:T(2,128)} %param.37) | copy-start | bytes 388
  37.6 40.0 %copy-start.8 = (bf16[16,256]{1,0:T(8,128)(2,1)S(1)}, bf16[16,256]{1,0:T(8,128)(2,1)}, u32[]{:S(2)}) copy-start(bf16[16,256]{1,0:T(8,128)(2,1)} %param.23) | copy-start | bytes 24580
  37.6 54.8 %copy-start.6 = (f32[2048]{0:T(1024)S(1)}, f32[2048]{0:T(1024)}, u32[]{:S(2)}) copy-start(f32[2048]{0:T(1024)} %param.35) | copy-start | bytes 24580
  38.8 67.3 %copy-start.7 = (bf16[16,2,128]{2,1,0:T(2,128)(2,1)}, bf16[16,2,128]{2,1,0:T(2,128)(2,1)S(1)}, u32[]{:S(2)}) copy-start(bf16[16,2,128]{2,1,0:T(2,128)(2,1)S(1)} %convert_element_type.102) | copy-start | bytes 24580
  38.8 67.3 %copy-start.1 = (bf16[256,2048]{1,0:T(8,128)(2,1)S(1)}, bf16[256,2048]{1,0:T(8,128)(2,1)}, u32[]{:S(2)}) copy-start(bf16[256,2048]{1,0:T(8,128)(2,1)} %param.44) | copy-start | bytes 3145732
  38.8 67.3 %copy-start.2 = (bf16[2048,256]{1,0:T(8,128)(2,1)S(1)}, bf16[2048,256]{1,0:T(8,128)(2,1)}, u32[]{:S(2)}) copy-start(bf16[2048,256]{1,0:T(8,128)(2,1)} %param.43) | copy-start | bytes 3145732
  38.9 99.9 %copy-start.13 = (f32[256]{0:T(256)S(1)}, f32[256]{0:T(256)}, u32[]{:S(2)}) copy-start(f32[256]{0:T(256)} %param.45) | copy-start | bytes 3076
  47.0 46.2 %all-to-all-start.1 = ((bf16[4,8,4]{1,2,0:T(4,128)(2,1)}), bf16[4,8,4]{1,2,0:T(4,128)(2,1)S(1)}, u32[]{:S(2)}, u32[]{:S(2)}) async-start(bf16[4,8,4]{1,2,0:T(4,128)(2,1)} %copy.49), calls=%async_computation.2 | async-start | bytes 8192 | tf_op jit(solution)/shard_map/all_to_all | solution.py:128
  93.2 8.7 %all-to-all-start = ((bf16[4,8,2048]{2,1,0:T(8,128)(2,1)}), bf16[4,8,2048]{2,1,0:T(8,128)(2,1)S(1)}, u32[]{:S(2)}, u32[]{:S(2)}) async-start(bf16[4,8,2048]{2,1,0:T(8,128)(2,1)} %fusion), calls=%async_computation.1 | async-start | bytes 262144 | tf_op jit(solution)/shard_map/all_to_all | solution.py:127
  96.9 36.9 %reduce-scatter.6.cloned.1.call-start = ((), (), s32[]{:S(2)}) async-start(), calls=%async_computation.7 | async-start | bytes 294912 | tf_op jit(solution)/shard_map/reduce_scatter | solution.py:145
  106.1 58.6 %reduce-scatter.8.cloned.1.call-start = ((), (), s32[]{:S(2)}) async-start(), calls=%async_computation.8 | async-start | bytes 147456 | tf_op jit(solution)/shard_map/reduce_scatter | solution.py:146
  135.1 29.6 %all-to-all-start.2 = ((bf16[4,8,256]{2,1,0:T(8,128)(2,1)}), bf16[4,8,256]{2,1,0:T(8,128)(2,1)S(1)}, u32[]{:S(2)}, u32[]{:S(2)}) async-start(bf16[4,8,256]{2,1,0:T(8,128)(2,1)} %convert_bitcast_fusion), calls=%async_computation.4 | async-start | bytes 32768 | tf_op jit(solution)/shard_map/all_to_all | solution.py:148
Sparse Core Ops, SparseCore 0:
  45.9 31.5 reduce-scatter.3
  106.2 27.4 reduce-scatter.5
  136.0 28.7 reduce-scatter.7
where the time goes:
time: 174 us; the launch traced here: 173 us
  waiting for transfers between devices  83.8 us (48%)
  blocking collectives  29.8 us (17%)
  matrix products  24.9 us (14%)
  between operations  14 us (8%)
  starting transfers between devices  11 us (6%)
  other arithmetic  7.35 us (4%)
  local copies, waits for them, and re-layouts  1.82 us (1%)
    reduce_scatter x1, waiting for transfers between devices, body(): lax.psum_scatter(partial_value, 'tp', scatter_dimension=1, tiled=True)  26.8 us
    reduce_scatter x1, waiting for transfers between devices, body(): lax.psum_scatter(expert_part, 'tp', scatter_dimension=1, tiled=True)  26.1 us
    reduce_scatter x1, waiting for transfers between devices, body(): lax.psum_scatter(dense_part, 'tp', scatter_dimension=1, tiled=True)  26 us
    all_gather x1, blocking collectives, body(): gathered = lax.all_gather(tokens, 'tp', axis=1, tiled=True)  15.9 us
    all_gather x1, blocking collectives, body(): lax.all_gather(own_residual, 'tp', axis=1, tiled=True)  13.9 us
    dot_general x1, matrix products, attend(): jnp.einsum('shd,shld->shl', queries, key_cache, preferred_element_type=jn...  5.63 us
    all_to_all x1, waiting for transfers between devices, body(): lax.all_to_all(send_rows, 'ep', split_axis=0, concat_axis=0, tiled=True)  4.85 us
    dot_general x1, matrix products, attend(): jnp.einsum('shl,shld->shd', weights, value_cache, preferred_element_type=...  4.72 us
  transfers between devices with their start and end apart: 6, of which 4 were waited for; matrix products, arithmetic and copies ran while one was open for 3% of the time, Pallas kernels for 0%

commit v1 on v0

--- a/solution.py
+++ b/solution.py
@@ -7,6 +7,19 @@
 EPG = 4
 EPS = 1e-06
 FLOOR = -1e30
+
+
+def gather_around(x, axis, dim):
+    ways = lax.axis_size(axis)
+    up = [(d, (d + 1) % ways) for d in range(ways)]
+    down = [(d, (d - 1) % ways) for d in range(ways)]
+    earlier, later = ([x], [x])
+    for _ in range(ways // 2):
+        earlier.append(lax.ppermute(earlier[-1], axis, up))
+    for _ in range((ways - 1) // 2):
+        later.append(lax.ppermute(later[-1], axis, down))
+    line = jnp.concatenate([*earlier[::-1], *later[1:]], axis=dim)
+    return jnp.roll(line, (lax.axis_index(axis) - ways // 2) * x.shape[dim], axis=dim)
 
 
 def norm_rows(row_data, gain_vec):
@@ -104,7 +117,7 @@
     )
     piece_sum = lax.psum_scatter(partial_value, "tp", scatter_dimension=1, tiled=True)
     own_residual = (tokens.astype(jnp.float32) + piece_sum).astype(jnp.bfloat16)
-    moe_in = norm_rows(lax.all_gather(own_residual, "tp", axis=1, tiled=True), moe_gain)
+    moe_in = norm_rows(gather_around(own_residual, "tp", 1), moe_gain)
     groups = lax.axis_size("ep")
     capacity = max(2, 2 * seq_count // groups)
     first_share = jax.nn.sigmoid(pair_logits[:, 0] - pair_logits[:, 1])

time: 174 us -> 183 us (1.052)
  blocking collectives: 29.8 us -> 15.9 us
  waiting for transfers between devices: 83.8 us -> 97.2 us
  starting transfers between devices: 11 us -> 21.6 us
    all_gather x1 -> x0, blocking collectives: 13.9 us -> none  [body(): lax.all_gather(own_residual, 'tp', axis=1, tiled=True)]
    ppermute x0 -> x7, starting transfers between devices: none -> 10.4 us  [the longest x3 10.4 us: gather_around(): later.append(lax.ppermute(later[-1], axis, down))]
    ppermute x0 -> x7, waiting for transfers between devices: none -> 8.76 us  [the longest x4 6.12 us: gather_around(): earlier.append(lax.ppermute(earlier[-1], axis, up))]
    reduce_scatter x1, waiting for transfers between devices: 26.8 us -> 31.4 us  [body(): lax.psum_scatter(partial_value, 'tp', scatter_dimension=1, tiled=True)]
  transfers between devices with their start and end apart: 6 -> 13, of which waited for: 4 -> 8; matrix products, arithmetic and copies ran while one was open for 3% -> 4% of each run, Pallas kernels for 0% -> 0%
where the time goes in v1:
time: 183 us; the launch traced here: 182 us
  waiting for transfers between devices  97.2 us (53%)
  matrix products  23.9 us (13%)
  starting transfers between devices  21.6 us (12%)
  blocking collectives  15.9 us (9%)
  between operations  14.1 us (8%)
  other arithmetic  7.3 us (4%)
  local copies, waits for them, and re-layouts  1.85 us (1%)
    reduce_scatter x1, waiting for transfers between devices, body(): lax.psum_scatter(partial_value, 'tp', scatter_dimension=1, tiled=True)  31.4 us
    reduce_scatter x1, waiting for transfers between devices, body(): lax.psum_scatter(expert_part, 'tp', scatter_dimension=1, tiled=True)  26.1 us
    reduce_scatter x1, waiting for transfers between devices, body(): lax.psum_scatter(dense_part, 'tp', scatter_dimension=1, tiled=True)  26 us
    all_gather x1, blocking collectives, body(): gathered = lax.all_gather(tokens, 'tp', axis=1, tiled=True)  15.9 us
    ppermute x3, starting transfers between devices, gather_around(): later.append(lax.ppermute(later[-1], axis, down))  10.4 us
    ppermute x4, waiting for transfers between devices, gather_around(): earlier.append(lax.ppermute(earlier[-1], axis, up))  6.12 us
    dot_general x1, matrix products, attend(): jnp.einsum('shd,shld->shl', queries, key_cache, preferred_element_type=jn...  5.63 us
    all_to_all x1, waiting for transfers between devices, body(): lax.all_to_all(send_rows, 'ep', split_axis=0, concat_axis=0, tiled=True)  4.85 us
  transfers between devices with their start and end apart: 13, of which 8 were waited for; matrix products, arithmetic and copies ran while one was open for 4% of the time, Pallas kernels for 0%

profile of v1, /device:TPU:0, one launch (start us, length us, event | category | flops | bytes accessed | tf_op | source)
XLA Modules:
  0.0 181.9 jit_solution(3520858285360557099)
XLA Ops:
  7.3 0.8 broadcast_add_fusion
  8.0 0.7 iota_compare_fusion.1
  8.7 15.9 %all_gather.3 = bf16[16,2048]{1,0:T(8,128)(2,1)S(1)} all-gather(bf16[16,256]{1,0:T(8,128)(2,1)} %param.23), channel_id=1, replica_groups=mesh['ep'=4,'tp'=8] {'tp'}, dimensions={1}, use_global_device_ids=true | all-gather | bytes 73728 | tf_op jit(solution)/shard_map/all_gather | solution.py:87
  24.8 1.5 fusion.70
  26.4 1.5 fusion.73
  28.1 1.1 select_reduce_fusion
  29.3 0.7 dynamic_slice.11
  30.0 1.0 fusion.58
  31.1 0.7 multiply_reduce_fusion
  31.8 5.6 %fusion.34 = f32[16,2,1,1024]{3,2,1,0:T(1,128)S(1)} fusion(bf16[16,2,1024,128]{3,2,1,0:T(8,128)(2,1)} %param.24, bf16[16,2,128,1]{2,1,0,3:T(2,128)(2,1)S(1)} %get-tuple-element.12), kind=kOutput, calls=%fused_computation.64 | convolution fusion | flops 8388608 | bytes 8527872 | tf_op jit(solution)/shard_map/shd,shld->shl/dot_general | solution.py:39
  38.8 4.6 %fusion.24 = f32[16,2,1,128]{3,2,1,0:T(1,128)S(1)} fusion(bf16[16,2,1024,128]{3,2,1,0:T(8,128)(2,1)} %param.25, bf16[16,2,1024,1]{2,1,0,3:T(2,128)(2,1)S(1)} %fusion.26), kind=kOutput, calls=%fused_computation.33 | convolution fusion | flops 8388608 | bytes 8470528 | tf_op jit(solution)/shard_map/shl,shld->shd/dot_general | solution.py:55
  43.5 0.9 fusion.39
  44.7 31.4 %reduce-scatter.4.cloned.1.call-done = f32[16,256]{1,0:T(8,128)} async-done(((f32[16,2048]{1,0:T(8,128)}), f32[16,256]{1,0:T(8,128)}) %reduce-scatter.4.cloned.1.call-update) | async-done | bytes 16400 | tf_op jit(solution)/shard_map/reduce_scatter | solution.py:118
  76.1 0.7 add_convert_fusion
  76.9 4.8 %collective-permute-done = bf16[16,256]{1,0:T(8,128)(2,1)S(1)} collective-permute-done((bf16[16,256]{1,0:T(8,128)(2,1)S(1)}, bf16[16,256]{1,0:T(8,128)(2,1)S(1)}, u32[]{:S(2)}, u32[]{:S(2)}) %collective-permute-start) | collective-permute-done | bytes 8224 | tf_op jit(solution)/shard_map/ppermute | solution.py:18
  81.7 3.6 %collective-permute-start.4 = (bf16[16,256]{1,0:T(8,128)(2,1)S(1)}, bf16[16,256]{1,0:T(8,128)(2,1)S(1)}, u32[]{:S(2)}, u32[]{:S(2)}) collective-permute-start(bf16[16,256]{1,0:T(8,128)(2,1)S(1)} %add_convert_fusion), channel_id=1, source_target_pairs={{0,7},{1,0},{2,1},{3,2},{4,3},{5,4},{6,5},{7,6},{8,15},{9,8},{10,9... | collective-permute-start | bytes 24584 | tf_op jit(solution)/shard_map/ppermute | solution.py:20
  85.3 1.3 collective-permute-done.1
  87.4 3.6 %all-to-all-start.1 = ((bf16[4,8,4]{1,2,0:T(4,128)(2,1)}), bf16[4,8,4]{1,2,0:T(4,128)(2,1)S(1)}, u32[]{:S(2)}, u32[]{:S(2)}) async-start(bf16[4,8,4]{1,2,0:T(4,128)(2,1)} %copy.49), calls=%async_computation.2 | async-start | bytes 8192 | tf_op jit(solution)/shard_map/all_to_all | solution.py:141
  91.1 3.3 %collective-permute-start.5 = (bf16[16,256]{1,0:T(8,128)(2,1)S(1)}, bf16[16,256]{1,0:T(8,128)(2,1)S(1)}, u32[]{:S(2)}, u32[]{:S(2)}) collective-permute-start(bf16[16,256]{1,0:T(8,128)(2,1)S(1)} %collective-permute-done.4), channel_id=1, source_target_pairs={{0,7},{1,0},{2,1},{3,2},{4,3},{5,4},{6,5},{7,6},{8,15},{9,8},{10,9... | collective-permute-start | bytes 24584 | tf_op jit(solution)/shard_map/ppermute | solution.py:20
  94.4 1.3 collective-permute-done.5
  95.7 3.5 %collective-permute-start.6 = (bf16[16,256]{1,0:T(8,128)(2,1)S(1)}, bf16[16,256]{1,0:T(8,128)(2,1)S(1)}, u32[]{:S(2)}, u32[]{:S(2)}) collective-permute-start(bf16[16,256]{1,0:T(8,128)(2,1)S(1)} %collective-permute-done.5), channel_id=1, source_target_pairs={{0,7},{1,0},{2,1},{3,2},{4,3},{5,4},{6,5},{7,6},{8,15},{9,8},{10,9... | collective-permute-start | bytes 24584 | tf_op jit(solution)/shard_map/ppermute | solution.py:20
  99.3 1.3 collective-permute-done.6
  100.8 0.9 fusion
  101.7 3.9 %all-to-all-start = ((bf16[4,8,2048]{2,1,0:T(8,128)(2,1)}), bf16[4,8,2048]{2,1,0:T(8,128)(2,1)S(1)}, u32[]{:S(2)}, u32[]{:S(2)}) async-start(bf16[4,8,2048]{2,1,0:T(8,128)(2,1)} %fusion), calls=%async_computation.1 | async-start | bytes 262144 | tf_op jit(solution)/shard_map/all_to_all | solution.py:140
  105.7 4.8 %all-to-all-done = bf16[4,8,2048]{2,1,0:T(8,128)(2,1)S(1)} async-done(((bf16[4,8,2048]{2,1,0:T(8,128)(2,1)}), bf16[4,8,2048]{2,1,0:T(8,128)(2,1)S(1)}, u32[]{:S(2)}, u32[]{:S(2)}) %all-to-all-start) | async-done | bytes 131104 | tf_op jit(solution)/shard_map/all_to_all | solution.py:140
  110.9 2.7 %fusion.4 = f32[32,2048]{1,0:T(8,128)} fusion(bf16[1,256,2048]{2,1,0:T(8,128)(2,1)S(1)} %copy-done, bf16[1,2048,256]{2,1,0:T(8,128)(2,1)} %param.41, bf16[4,8,2048]{2,1,0:T(8,128)(2,1)S(1)} %all-to-all-done, f32[32,256]{1,0:T(8,128)S(1)} %fusion.10, f32[32]{0:T(128)S(1)} %mul.185), kind=kOutput, calls=%fused_computation.7 | convolution fusion | flops 67166208 | bytes 2523264 | tf_op jit(solution)/shard_map/dot_general | solution.py:156
  113.6 3.0 %fusion.38 = f32[16,2048]{1,0:T(8,128)} fusion(bf16[256,2048]{1,0:T(8,128)(2,1)} %param.44, bf16[2048,256]{1,0:T(8,128)(2,1)} %param.43, f32[2048]{0:T(1024)S(1)} %copy-done.6, f32[16]{0:T(128)S(1)} %add_rsqrt_fusion.2, bf16[16,4096]{1,0:T(8,128)(2,1)S(1)} %constant_dynamic-update-slice_fusion, s32[]{:T(128)S(6)} %select_n.51), kind=kOutput, calls=%fused_computation.78 | convolution fusion | flops 33705984 | bytes 2302468 | tf_op jit(solution)/shard_map/dot_general | solution.py:146
  116.7 26.1 %reduce-scatter.6.cloned.1.call-done = f32[32,256]{1,0:T(8,128)} async-done(((f32[32,2048]{1,0:T(8,128)}), f32[32,256]{1,0:T(8,128)}) %reduce-scatter.6.cloned.1.call-update) | async-done | bytes 32784 | tf_op jit(solution)/shard_map/reduce_scatter | solution.py:158
  142.8 1.4 convert_bitcast_fusion
  144.2 3.7 %all-to-all-start.2 = ((bf16[4,8,256]{2,1,0:T(8,128)(2,1)}), bf16[4,8,256]{2,1,0:T(8,128)(2,1)S(1)}, u32[]{:S(2)}, u32[]{:S(2)}) async-start(bf16[4,8,256]{2,1,0:T(8,128)(2,1)} %convert_bitcast_fusion), calls=%async_computation.4 | async-start | bytes 32768 | tf_op jit(solution)/shard_map/all_to_all | solution.py:161
  147.8 26.0 %reduce-scatter.8.cloned.1.call-done = f32[16,256]{1,0:T(8,128)} async-done(((f32[16,2048]{1,0:T(8,128)}), f32[16,256]{1,0:T(8,128)}) %reduce-scatter.8.cloned.1.call-update) | async-done | bytes 16400 | tf_op jit(solution)/shard_map/reduce_scatter | solution.py:159
  173.8 1.5 fusion.5
  (96 shorter events, 3.9 us)
Async XLA Ops:
  7.2 103.7 %copy-start = (bf16[1,256,2048]{2,1,0:T(8,128)(2,1)S(1)}, bf16[1,256,2048]{2,1,0:T(8,128)(2,1)}, u32[]{:S(2)}) copy-start(bf16[1,256,2048]{2,1,0:T(8,128)(2,1)} %param.42) | copy-start | bytes 3145732
  7.2 31.3 %copy-start.5 = (f32[2048]{0:T(1024)S(1)}, f32[2048]{0:T(1024)}, u32[]{:S(2)}) copy-start(f32[2048]{0:T(1024)} %param.28) | copy-start | bytes 24580
  7.2 30.3 %copy-start.4 = (f32[16,2,1024]{2,1,0:T(2,128)S(1)}, f32[16,2,1024]{2,1,0:T(2,128)}, u32[]{:S(2)}) copy-start(f32[16,2,1024]{2,1,0:T(2,128)} %param.26) | copy-start | bytes 393220
  7.2 68.9 %reduce-scatter.4.cloned.1.call-start = ((), (), s32[]{:S(2)}) async-start(), calls=%async_computation.6 | async-start | bytes 147456 | tf_op jit(solution)/shard_map/reduce_scatter | solution.py:118
  31.0 12.3 %copy-start.11 = (f32[16,2]{0,1:T(2,128)}, f32[16,2]{0,1:T(2,128)S(1)}, u32[]{:S(2)}) copy-start(f32[16,2]{0,1:T(2,128)S(1)} %fusion.58) | copy-start | bytes 388
  31.1 7.3 %copy-start.3 = (bf16[2048,256]{1,0:T(8,128)(2,1)S(1)}, bf16[2048,256]{1,0:T(8,128)(2,1)}, u32[]{:S(2)}) copy-start(bf16[2048,256]{1,0:T(8,128)(2,1)} %param.31) | copy-start | bytes 3145732
  37.5 6.0 %copy-start.1 = (bf16[256,2048]{1,0:T(8,128)(2,1)S(1)}, bf16[256,2048]{1,0:T(8,128)(2,1)}, u32[]{:S(2)}) copy-start(bf16[256,2048]{1,0:T(8,128)(2,1)} %param.34) | copy-start | bytes 3145732
  37.5 6.9 %copy-start.9 = (s32[16,1]{0,1:T(1,128)S(1)}, s32[16,1]{0,1:T(1,128)}, u32[]{:S(2)}) copy-start(s32[16,1]{0,1:T(1,128)} %param.36) | copy-start | bytes 196
  37.5 7.2 %copy-start.12 = (f32[16,2]{0,1:T(2,128)S(1)}, f32[16,2]{0,1:T(2,128)}, u32[]{:S(2)}) copy-start(f32[16,2]{0,1:T(2,128)} %param.39) | copy-start | bytes 388
  37.5 38.6 %copy-start.8 = (bf16[16,256]{1,0:T(8,128)(2,1)S(1)}, bf16[16,256]{1,0:T(8,128)(2,1)}, u32[]{:S(2)}) copy-start(bf16[16,256]{1,0:T(8,128)(2,1)} %param.23) | copy-start | bytes 24580
  37.5 39.3 %copy-start.14 = (f32[16]{0:T(128)S(1)}, f32[16]{0:T(128)}, u32[]{:S(2)}) copy-start(f32[16]{0:T(128)} %param.38) | copy-start | bytes 196
  37.5 44.2 %copy-start.10 = (s32[16,2]{0,1:T(2,128)S(1)}, s32[16,2]{0,1:T(2,128)}, u32[]{:S(2)}) copy-start(s32[16,2]{0,1:T(2,128)} %param.37) | copy-start | bytes 388
  37.5 63.2 %copy-start.6 = (f32[2048]{0:T(1024)S(1)}, f32[2048]{0:T(1024)}, u32[]{:S(2)}) copy-start(f32[2048]{0:T(1024)} %param.35) | copy-start | bytes 24580
  37.9 72.7 %copy-start.2 = (bf16[1,2048,256]{2,1,0:T(8,128)(2,1)S(1)}, bf16[1,2048,256]{2,1,0:T(8,128)(2,1)}, u32[]{:S(2)}) copy-start(bf16[1,2048,256]{2,1,0:T(8,128)(2,1)} %param.40) | copy-start | bytes 3145732
  38.8 74.8 %copy-start.7 = (bf16[16,2,128]{2,1,0:T(2,128)(2,1)}, bf16[16,2,128]{2,1,0:T(2,128)(2,1)S(1)}, u32[]{:S(2)}) copy-start(bf16[16,2,128]{2,1,0:T(2,128)(2,1)S(1)} %convert_element_type.102) | copy-start | bytes 24580
  38.8 109.0 %copy-start.13 = (f32[256]{0:T(256)S(1)}, f32[256]{0:T(256)}, u32[]{:S(2)}) copy-start(f32[256]{0:T(256)} %param.45) | copy-start | bytes 3076
  76.9 4.9 %collective-permute-start = (bf16[16,256]{1,0:T(8,128)(2,1)S(1)}, bf16[16,256]{1,0:T(8,128)(2,1)S(1)}, u32[]{:S(2)}, u32[]{:S(2)}) collective-permute-start(bf16[16,256]{1,0:T(8,128)(2,1)S(1)} %add_convert_fusion), channel_id=1, source_target_pairs={{0,1},{1,2},{2,3},{3,4},{4,5},{5,6},{6,7},{7,0},{8,9},{9,10},{10,1... | collective-permute-start | bytes 24584 | tf_op jit(solution)/shard_map/ppermute | solution.py:18
  81.7 4.9 %collective-permute-start.1 = (bf16[16,256]{1,0:T(8,128)(2,1)S(1)}, bf16[16,256]{1,0:T(8,128)(2,1)S(1)}, u32[]{:S(2)}, u32[]{:S(2)}) collective-permute-start(bf16[16,256]{1,0:T(8,128)(2,1)S(1)} %collective-permute-done), channel_id=1, source_target_pairs={{0,1},{1,2},{2,3},{3,4},{4,5},{5,6},{6,7},{7,0},{8,9},{9,10},{10,1... | collective-permute-start | bytes 24584 | tf_op jit(solution)/shard_map/ppermute | solution.py:18
  81.7 9.3 %collective-permute-start.4 = (bf16[16,256]{1,0:T(8,128)(2,1)S(1)}, bf16[16,256]{1,0:T(8,128)(2,1)S(1)}, u32[]{:S(2)}, u32[]{:S(2)}) collective-permute-start(bf16[16,256]{1,0:T(8,128)(2,1)S(1)} %add_convert_fusion), channel_id=1, source_target_pairs={{0,7},{1,0},{2,1},{3,2},{4,3},{5,4},{6,5},{7,6},{8,15},{9,8},{10,9... | collective-permute-start | bytes 24584 | tf_op jit(solution)/shard_map/ppermute | solution.py:20
  86.6 7.7 %collective-permute-start.2 = (bf16[16,256]{1,0:T(8,128)(2,1)S(1)}, bf16[16,256]{1,0:T(8,128)(2,1)S(1)}, u32[]{:S(2)}, u32[]{:S(2)}) collective-permute-start(bf16[16,256]{1,0:T(8,128)(2,1)S(1)} %collective-permute-done.1), channel_id=1, source_target_pairs={{0,1},{1,2},{2,3},{3,4},{4,5},{5,6},{6,7},{7,0},{8,9},{9,10},{10,1... | collective-permute-start | bytes 24584 | tf_op jit(solution)/shard_map/ppermute | solution.py:18
  87.4 14.2 %all-to-all-start.1 = ((bf16[4,8,4]{1,2,0:T(4,128)(2,1)}), bf16[4,8,4]{1,2,0:T(4,128)(2,1)S(1)}, u32[]{:S(2)}, u32[]{:S(2)}) async-start(bf16[4,8,4]{1,2,0:T(4,128)(2,1)} %copy.49), calls=%async_computation.2 | async-start | bytes 8192 | tf_op jit(solution)/shard_map/all_to_all | solution.py:141
  91.1 4.6 %collective-permute-start.5 = (bf16[16,256]{1,0:T(8,128)(2,1)S(1)}, bf16[16,256]{1,0:T(8,128)(2,1)S(1)}, u32[]{:S(2)}, u32[]{:S(2)}) collective-permute-start(bf16[16,256]{1,0:T(8,128)(2,1)S(1)} %collective-permute-done.4), channel_id=1, source_target_pairs={{0,7},{1,0},{2,1},{3,2},{4,3},{5,4},{6,5},{7,6},{8,15},{9,8},{10,9... | collective-permute-start | bytes 24584 | tf_op jit(solution)/shard_map/ppermute | solution.py:20
  94.3 4.9 %collective-permute-start.3 = (bf16[16,256]{1,0:T(8,128)(2,1)S(1)}, bf16[16,256]{1,0:T(8,128)(2,1)S(1)}, u32[]{:S(2)}, u32[]{:S(2)}) collective-permute-start(bf16[16,256]{1,0:T(8,128)(2,1)S(1)} %collective-permute-done.2), channel_id=1, source_target_pairs={{0,1},{1,2},{2,3},{3,4},{4,5},{5,6},{6,7},{7,0},{8,9},{9,10},{10,1... | collective-permute-start | bytes 24584 | tf_op jit(solution)/shard_map/ppermute | solution.py:18
  95.7 4.9 %collective-permute-start.6 = (bf16[16,256]{1,0:T(8,128)(2,1)S(1)}, bf16[16,256]{1,0:T(8,128)(2,1)S(1)}, u32[]{:S(2)}, u32[]{:S(2)}) collective-permute-start(bf16[16,256]{1,0:T(8,128)(2,1)S(1)} %collective-permute-done.5), channel_id=1, source_target_pairs={{0,7},{1,0},{2,1},{3,2},{4,3},{5,4},{6,5},{7,6},{8,15},{9,8},{10,9... | collective-permute-start | bytes 24584 | tf_op jit(solution)/shard_map/ppermute | solution.py:20
  101.7 8.9 %all-to-all-start = ((bf16[4,8,2048]{2,1,0:T(8,128)(2,1)}), bf16[4,8,2048]{2,1,0:T(8,128)(2,1)S(1)}, u32[]{:S(2)}, u32[]{:S(2)}) async-start(bf16[4,8,2048]{2,1,0:T(8,128)(2,1)} %fusion), calls=%async_computation.1 | async-start | bytes 262144 | tf_op jit(solution)/shard_map/all_to_all | solution.py:140
  105.6 37.2 %reduce-scatter.6.cloned.1.call-start = ((), (), s32[]{:S(2)}) async-start(), calls=%async_computation.7 | async-start | bytes 294912 | tf_op jit(solution)/shard_map/reduce_scatter | solution.py:158
  113.6 60.2 %reduce-scatter.8.cloned.1.call-start = ((), (), s32[]{:S(2)}) async-start(), calls=%async_computation.8 | async-start | bytes 147456 | tf_op jit(solution)/shard_map/reduce_scatter | solution.py:159
  144.2 29.7 %all-to-all-start.2 = ((bf16[4,8,256]{2,1,0:T(8,128)(2,1)}), bf16[4,8,256]{2,1,0:T(8,128)(2,1)S(1)}, u32[]{:S(2)}, u32[]{:S(2)}) async-start(bf16[4,8,256]{2,1,0:T(8,128)(2,1)} %convert_bitcast_fusion), calls=%async_computation.4 | async-start | bytes 32768 | tf_op jit(solution)/shard_map/all_to_all | solution.py:161
Sparse Core Ops, SparseCore 0:
  44.5 31.5 reduce-scatter.3
  113.7 29.0 reduce-scatter.5
  145.1 28.7 reduce-scatter.7
